TPU v7x, 512 devices: a whole 4x8x8 slice. The times are simulated.
512 devices in a mesh: sp: 32 (over z, x), tp: 16 (over y, core).
Axes of the slice: x: 4, y: 8, z: 8, core: 2. Of those that a mesh axis runs over, the one named last changes fastest.
Arguments:
- lane_source_signal: bfloat16 [1024, 4096], P('tp', 'sp'), may hold values from -6 to 6
- spectral_damping_part: float32 [64, 64], P('tp'), may hold values from -3 to -0.0002
- spectral_angular_part: float32 [64, 64], P('tp'), may hold values from 0.31 to 201.0624
- interval_exponent: float32 [64], P('tp'), may hold values from -3.9 to -1.6
- entry_matrix_inphase: float32 [64, 64, 16], P('tp'), may hold values from -1 to 1
- entry_matrix_quadrature: float32 [64, 64, 16], P('tp'), may hold values from -1 to 1
- emission_inphase: float32 [64, 16, 64], P('tp'), may hold values from -0.75 to 0.75
- emission_quadrature: float32 [64, 16, 64], P('tp'), may hold values from -0.75 to 0.75
- lane_bypass_factor: float32 [1024], P('tp'), may hold values from -5 to 5
- spike_shrink_offset: float32 [64, 4096], P('tp', 'sp'), may hold values from -1.4 to 0
- lane_exit_matrix: bfloat16 [1024, 4096], P('tp'), may hold values from -0.1875 to 0.1875
- skipline_stream: bfloat16 [4096, 4096], P('sp'), may hold values from -6 to 6
- specialist_scaling_vector: float32 [4096], replicated, may hold values from 0.1 to 1.9
- selected_specialists: int32 [4096, 2], P('sp'), may hold values from 0 to 31, all different within a row; in each aligned block of 128 rows (0 to 127, 128 to 255, ...) at most 16 rows name the same one
- dispatcher_scores: float32 [4096, 2], P('sp'), may hold values from 0.1 to 1
- specialist_valve_matrix: bfloat16 [32, 4096, 2048], P('sp', None, 'tp'), may hold values from -0.09375 to 0.09375
- specialist_widen_matrix: bfloat16 [32, 4096, 2048], P('sp', None, 'tp'), may hold values from -0.09375 to 0.09375
- specialist_shrink_matrix: bfloat16 [32, 2048, 4096], P('sp', 'tp'), may hold values from -0.1875 to 0.1875
Outputs:
- updated: bfloat16 [4096, 4096], P('sp', 'tp')
Inputs may be any that keep to these rules, and one draw needn't show every extreme that they name: `selected_specialists`: each row names 2 different experts. Among the rows of each aligned block of 128 positions no expert is named more than 16 times, and in every block some expert is named exactly 16 times.
All inputs are finite; a program needn't handle non-finite values.
Results may differ from a plain program's by a relative error of at most 0.019.
Values may be sent and summed in bfloat16 or wider, within the bound.
A program may use at most 64 MiB of HBM per device.

v0:
```python
import jax
import jax.numpy as jnp
from jax import lax
from jax.sharding import PartitionSpec as P

EPS = 1e-06
PRECISE_MODE = lax.Precision.HIGHEST


def copy_for_each(array, axis):
    copies = jnp.broadcast_to(array, (lax.axis_size(axis), *array.shape))
    return lax.all_to_all(copies, axis, split_axis=0, concat_axis=0, tiled=True)


def gathered_once(array, axis):
    leaves = jax.tree.leaves(array)
    order = sorted(range(len(leaves)), key=lambda k: -leaves[k].size)
    width = (1, *leaves[order[0]].shape)[-1]
    lines = [
        jnp.pad(leaves[k].reshape(-1), (0, -leaves[k].size % width)).reshape(-1, width)
        for k in order
    ]
    both, at, found = (copy_for_each(jnp.concatenate(lines), axis), 0, {})
    for k, line in zip(order, lines):
        share = both[:, at : at + len(line)].reshape(len(both), -1)
        found[k] = share[:, : leaves[k].size].reshape(-1, *leaves[k].shape)
        at += len(line)
    numbers = iter(range(len(leaves)))
    return jax.tree.map(lambda _: found[next(numbers)], array)


def combined_pairwise(pieces, combine):
    while len(jax.tree.leaves(pieces)[0]) > 1:
        pieces = jax.vmap(combine)(
            *(jax.tree.map(lambda part: part[side::2], pieces) for side in (0, 1))
        )
    return jax.tree.map(lambda part: part[0], pieces)


def prefix(array, axis, combine, identity):
    length, mine = (lax.axis_size(axis), lax.axis_index(axis))
    passed = jnp.arange(length) < mine

    def kept(part, zero, own):
        part = jnp.where(
            passed.reshape(-1, *(1 for _ in own.shape)), part, jnp.asarray(zero, own.dtype)
        )
        return part

    pieces = gathered_once(array, axis)
    return combined_pairwise(jax.tree.map(kept, pieces, identity, array), combine)


def in_blocks(array, dim, length):
    before, after = (array.shape[:dim], array.shape[dim + 1 :])
    return jnp.moveaxis(array.reshape(*before, length, -1, *after), dim, 0)


def sent_and_summed(array, axis, dim):
    length = lax.axis_size(axis)
    parts = lax.all_to_all(in_blocks(array, dim, length), axis, 0, 0, tiled=True)
    return jnp.sum(parts.astype(jnp.float32), axis=0)


def taken_together(array, axis):
    return copy_for_each(array, axis).sum(axis=0)


def affine_pair(earlier, latter):
    mul_re = earlier[0] * latter[0] - earlier[1] * latter[1]
    mul_im = earlier[0] * latter[1] + earlier[1] * latter[0]
    add_re = latter[0] * earlier[2] - latter[1] * earlier[3] + latter[2]
    add_im = latter[0] * earlier[3] + latter[1] * earlier[2] + latter[3]
    return (mul_re, mul_im, add_re, add_im)


def local_prefix(elements):
    length = elements[0].shape[2]
    fills = (1.0, 0.0, 0.0, 0.0)
    offset = 1
    while offset < length:
        earlier = tuple(
            (
                jnp.pad(
                    item[:, :, : length - offset],
                    ((0, 0), (0, 0), (offset, 0)),
                    constant_values=fill,
                )
                for item, fill in zip(elements, fills)
            )
        )
        elements = affine_pair(earlier, elements)
        offset = offset * 2
    return elements


def per_device(
    lane_source_signal,
    spectral_damping_part,
    spectral_angular_part,
    interval_exponent,
    entry_matrix_inphase,
    entry_matrix_quadrature,
    emission_inphase,
    emission_quadrature,
    lane_bypass_factor,
    spike_shrink_offset,
    lane_exit_matrix,
    skipline_stream,
    specialist_scaling_vector,
    selected_specialists,
    dispatcher_scores,
    specialist_valve_matrix,
    specialist_widen_matrix,
    specialist_shrink_matrix,
):
    f32 = jnp.float32
    bf16 = jnp.bfloat16
    groups_here = spectral_damping_part.shape[0]
    lanes_within_bundle = entry_matrix_inphase.shape[2]
    tok_local = lane_source_signal.shape[1]
    bundled_signal = lane_source_signal.astype(f32).reshape(
        groups_here, lanes_within_bundle, tok_local
    )
    step_size = jnp.exp(interval_exponent)[:, None]
    natural_pace_exponent = spectral_damping_part * step_size
    angle = spectral_angular_part * step_size
    num_re = jnp.expm1(natural_pace_exponent) * jnp.cos(angle) - 2.0 * jnp.sin(0.5 * angle) ** 2
    num_im = jnp.exp(natural_pace_exponent) * jnp.sin(angle)
    denom = (
        spectral_damping_part * spectral_damping_part
        + spectral_angular_part * spectral_angular_part
    )
    fac_re = (num_re * spectral_damping_part + num_im * spectral_angular_part) / denom
    fac_im = (num_im * spectral_damping_part - num_re * spectral_angular_part) / denom
    map_re = (
        fac_re[:, :, None] * entry_matrix_inphase - fac_im[:, :, None] * entry_matrix_quadrature
    )
    map_im = (
        fac_re[:, :, None] * entry_matrix_quadrature + fac_im[:, :, None] * entry_matrix_inphase
    )
    drive_re = jnp.einsum("gpc,gct->gpt", map_re, bundled_signal, precision=PRECISE_MODE)
    drive_im = jnp.einsum("gpc,gct->gpt", map_im, bundled_signal, precision=PRECISE_MODE)
    recurrence_modulus = jnp.exp(
        natural_pace_exponent[:, :, None] + spike_shrink_offset[:, None, :]
    )
    trans_re = recurrence_modulus * jnp.cos(angle)[:, :, None]
    trans_im = recurrence_modulus * jnp.sin(angle)[:, :, None]
    cum_re, cum_im, state_real, state_imaginary = local_prefix(
        (trans_re, trans_im, drive_re, drive_im)
    )
    summary = (cum_re[:, :, -1], cum_im[:, :, -1], state_real[:, :, -1], state_imaginary[:, :, -1])
    unit = jnp.ones_like(summary[0])
    blank = jnp.zeros_like(summary[0])
    carried = prefix(summary, "sp", affine_pair, (unit, blank, blank, blank))
    enter_re = carried[2][:, :, None]
    enter_im = carried[3][:, :, None]
    state_real = state_real + cum_re * enter_re - cum_im * enter_im
    state_imaginary = state_imaginary + cum_re * enter_im + cum_im * enter_re
    value = (
        jnp.einsum("nef,nfi->nei", emission_inphase, state_real, precision=PRECISE_MODE)
        - jnp.einsum("nef,nfi->nei", emission_quadrature, state_imaginary, precision=PRECISE_MODE)
        + lane_bypass_factor.reshape(groups_here, lanes_within_bundle)[:, :, None] * bundled_signal
    )
    recurrence_result = (
        jax.nn.gelu(value).astype(bf16).reshape(groups_here * lanes_within_bundle, tok_local)
    )
    width = specialist_scaling_vector.shape[0]
    d_local = width // lax.axis_size("tp")
    col_start = lax.axis_index("tp") * d_local
    partial_rows = jnp.einsum(
        "ct,cd->td", recurrence_result, lane_exit_matrix, preferred_element_type=f32
    )
    projected_own = sent_and_summed(partial_rows.astype(jnp.bfloat16), "tp", 1).astype(bf16)
    own_residual = lax.dynamic_slice_in_dim(skipline_stream, col_start, d_local, 1)
    stream_own = (
        own_residual.astype(f32) + lax.optimization_barrier(projected_own).astype(f32)
    ).astype(bf16)
    own_stream = lax.optimization_barrier(stream_own).astype(f32)
    square_total = taken_together(jnp.sum(own_stream * own_stream, axis=1), "tp")
    inv_rms = lax.rsqrt(square_total / width + EPS)[:, None]
    own_gain = lax.dynamic_slice_in_dim(specialist_scaling_vector, col_start, d_local, 0)
    own_cols = (own_stream * inv_rms * own_gain).astype(bf16)
    share = dispatcher_scores / jnp.sum(dispatcher_scores, axis=1, keepdims=True)
    experts = lax.axis_size("sp")
    top = selected_specialists.shape[1]
    capacity = 2 * tok_local * top // experts
    flat_routes = selected_specialists.reshape(-1)
    hits = (flat_routes[:, None] == jnp.arange(experts, dtype=jnp.int32)[None, :]).astype(jnp.int32)
    ranks = jnp.sum((jnp.cumsum(hits, axis=0) - hits) * hits, axis=1)
    slot_ids = flat_routes * capacity + ranks
    slot_grid = jnp.arange(experts * capacity, dtype=jnp.int32)
    matched = slot_grid[:, None] == slot_ids[None, :]
    token_of = jnp.arange(tok_local * top, dtype=jnp.int32) // top
    slot_token = jnp.sum(jnp.where(matched, token_of[None, :], 0), axis=1)
    slot_live = jnp.any(matched, axis=1)
    gate_w = specialist_valve_matrix[0]
    up_w = specialist_widen_matrix[0]
    down_w = specialist_shrink_matrix[0]
    bf_zero = jnp.zeros((), bf16)
    dispatch = jnp.where(slot_live[:, None], own_cols[slot_token], bf_zero).reshape(
        experts, capacity, d_local
    )
    arrived = lax.all_to_all(dispatch, "sp", split_axis=0, concat_axis=0, tiled=True)
    piece = lax.all_gather(arrived, "tp", axis=2, tiled=True)
    gate_part = jnp.einsum("snd,df->snf", piece, gate_w, preferred_element_type=f32)
    up_part = jnp.einsum("snd,df->snf", piece, up_w, preferred_element_type=f32)
    hidden = (jax.nn.silu(gate_part) * up_part).astype(bf16)
    flat_hidden = hidden.reshape(experts * capacity, hidden.shape[2])
    down_part = jnp.dot(flat_hidden, down_w, preferred_element_type=f32).astype(bf16)
    summed = lax.psum_scatter(
        down_part.astype(f32).astype(jnp.bfloat16), "tp", scatter_dimension=1, tiled=True
    ).astype(jnp.float32)
    expert_out = summed.astype(bf16).reshape(experts, capacity, d_local)
    returned = lax.all_to_all(expert_out, "sp", split_axis=0, concat_axis=0, tiled=True).reshape(
        experts * capacity, d_local
    )
    picked = returned[slot_ids].reshape(tok_local, top, d_local)
    combined = jnp.sum(lax.optimization_barrier(picked).astype(f32) * share[:, :, None], axis=1)
    return (own_stream + combined).astype(bf16)


def solution(mesh):
    placed = (
        P("tp", "sp"),
        P("tp", None),
        P("tp", None),
        P("tp"),
        P("tp", None, None),
        P("tp", None, None),
        P("tp", None, None),
        P("tp", None, None),
        P("tp"),
        P("tp", "sp"),
        P("tp", None),
        P("sp", None),
        P(),
        P("sp", None),
        P("sp", None),
        P("sp", None, "tp"),
        P("sp", None, "tp"),
        P("sp", "tp", None),
    )
    return jax.shard_map(
        per_device, mesh=mesh, in_specs=placed, out_specs=P("sp", "tp"), check_vma=False
    )
```

profile of v0, /device:TPU:25, one launch (start us, length us, event | category | flops | bytes accessed | tf_op | source)
XLA Modules:
  0.0 256.6 jit_solution(5773878891755166815)
XLA Ops:
  6.5 0.7 exp.13
  7.3 0.8 fusion.57
  8.1 1.1 fusion.42
  9.2 1.1 fusion.46
  10.3 0.9 subtract_add_fusion.6
  11.2 1.0 add_add_fusion.5
  12.2 0.1 subtract_add_fusion.5
  12.3 0.2 add_add_fusion.4
  12.5 0.1 subtract_add_fusion.4
  12.7 0.2 add_add_fusion.3
  12.9 0.1 subtract_add_fusion.3
  13.1 0.2 add_add_fusion.2
  13.3 0.1 subtract_add_fusion.2
  13.4 0.2 add_add_fusion.1
  13.7 0.1 subtract_add_fusion.1
  13.8 0.2 add_add_fusion
  14.0 0.2 multiply_subtract_fusion
  14.2 0.3 slice_reduce_fusion.1
  14.5 0.3 slice_reduce_fusion
  14.8 0.8 reshape.198
  15.6 12.9 %all-to-all-start = ((f32[32,1,1024]{2,1,0:T(1,128)}), f32[32,1,1024]{2,1,0:T(1,128)S(1)}, u32[]{:S(2)}, u32[]{:S(2)}) async-start(f32[32,1,1024]{2,1,0:T(1,128)} %reshape.198), calls=%async_computation | async-start | bytes 262144 | tf_op jit(solution)/shard_map/all_to_all | solution.py:12
  28.6 9.2 %all-to-all-done = f32[32,1,1024]{2,1,0:T(1,128)S(1)} async-done(((f32[32,1,1024]{2,1,0:T(1,128)}), f32[32,1,1024]{2,1,0:T(1,128)S(1)}, u32[]{:S(2)}, u32[]{:S(2)}) %all-to-all-start) | async-done | bytes 131104 | tf_op jit(solution)/shard_map/all_to_all | solution.py:12
  37.9 0.5 broadcast.191
  38.4 0.9 reduce.12
  39.4 0.1 reshape.199
  39.5 0.1 slice_select_fusion.3
  39.7 0.3 fusion.16
  40.1 0.4 fusion.36
  40.5 0.4 convolution_convert_fusion.1
  40.9 1.1 copy.117
  42.0 9.1 %all-to-all-start.1 = ((bf16[16,128,256]{2,1,0:T(8,128)(2,1)}), bf16[16,128,256]{2,1,0:T(8,128)(2,1)S(1)}, u32[]{:S(2)}, u32[]{:S(2)}) async-start(bf16[16,128,256]{2,1,0:T(8,128)(2,1)} %bitcast.68), calls=%async_computation.1 | async-start | bytes 2097152 | tf_op jit(solution)/shard_map/all_to_all | solution.py:61
  51.2 0.1 copy.107
  51.3 0.1 eq.40
  51.4 0.1 reshape.168
  51.6 0.6 reduce-window.6
  52.2 0.2 slice_reduce_fusion.4
  52.4 0.1 fusion.41
  52.5 0.2 fusion.7
  52.7 0.2 select_reduce_fusion
  52.9 24.5 %all-to-all-done.1 = bf16[16,128,256]{2,1,0:T(8,128)(2,1)S(1)} async-done(((bf16[16,128,256]{2,1,0:T(8,128)(2,1)}), bf16[16,128,256]{2,1,0:T(8,128)(2,1)S(1)}, u32[]{:S(2)}, u32[]{:S(2)}) %all-to-all-start.1) | async-done | bytes 1048608 | tf_op jit(solution)/shard_map/all_to_all | solution.py:61
  77.4 0.1 reduce_sum.70
  77.5 0.9 add_convert_fusion
  78.4 0.1 fusion.8
  78.5 0.6 broadcast_in_dim.86
  79.1 5.2 %all-to-all-start.2 = ((f32[16,1,128]{2,1,0:T(1,128)}), f32[16,1,128]{2,1,0:T(1,128)S(1)}, u32[]{:S(2)}, u32[]{:S(2)}) async-start(f32[16,1,128]{2,1,0:T(1,128)} %broadcast_in_dim.86), calls=%async_computation.2 | async-start | bytes 16384 | tf_op jit(solution)/shard_map/all_to_all | solution.py:12
  84.4 0.8 dynamic_slice.7
  85.3 3.2 %all-to-all-done.2 = f32[16,1,128]{2,1,0:T(1,128)S(1)} async-done(((f32[16,1,128]{2,1,0:T(1,128)}), f32[16,1,128]{2,1,0:T(1,128)S(1)}, u32[]{:S(2)}, u32[]{:S(2)}) %all-to-all-start.2) | async-done | bytes 8224 | tf_op jit(solution)/shard_map/all_to_all | solution.py:12
  88.5 0.1 fusion.10
  88.6 2.0 gather_fusion
  90.6 0.1 broadcast_select_fusion
  90.7 15.2 %all_to_all.26 = bf16[32,16,256]{2,1,0:T(8,128)(2,1)} all-to-all(bf16[32,16,256]{2,1,0:T(8,128)(2,1)S(1)} %broadcast_select_fusion), channel_id=1, replica_groups=mesh['sp'=32,'tp'=16] {'sp'}, dimensions={0} | all-to-all | bytes 524288 | tf_op jit(solution)/shard_map/all_to_all | solution.py:204
  106.0 45.2 %all-gather.2.cloned.1.call-done = bf16[32,16,4096]{2,1,0:T(8,128)(2,1)} async-done(((bf16[32,16,256]{2,1,0:T(8,128)(2,1)}), bf16[32,16,4096]{2,1,0:T(8,128)(2,1)}) %all-gather.2.cloned.1.call-update) | async-done | bytes 4194320 | tf_op jit(solution)/shard_map/all_gather | solution.py:205
  151.2 3.6 %fusion.5 = f32[32,16,128]{2,1,0:T(8,128)S(1)} fusion(bf16[32,16,4096]{2,1,0:T(8,128)(2,1)} %all-gather.2.cloned.1.call-done, bf16[1,4096,128]{2,1,0:T(8,128)(2,1)S(1)} %copy-done.2), kind=kOutput, calls=%fused_computation.12 | convolution fusion | flops 536870912 | bytes 5505024 | tf_op jit(solution)/shard_map/snd,df->snf/dot_general | solution.py:206
  154.8 2.5 fusion
  157.3 3.2 %convolution_convert_fusion = bf16[512,4096]{1,0:T(8,128)(2,1)} fusion(bf16[512,128]{1,0:T(8,128)(2,1)S(1)} %bitcast.140, bf16[1,128,4096]{2,1,0:T(8,128)(2,1)S(1)} %copy-done), kind=kOutput, calls=%fused_computation.2 | convolution fusion | flops 538968064 | bytes 5373952 | tf_op jit(solution)/shard_map/dot_general | solution.py:210
  160.5 0.1 copy.111
  160.6 0.1 mul.645
  160.8 65.8 %reduce-scatter.2.cloned.1.call-done = bf16[512,256]{1,0:T(8,128)(2,1)} async-done(((bf16[512,4096]{1,0:T(8,128)(2,1)}), bf16[512,256]{1,0:T(8,128)(2,1)}) %reduce-scatter.2.cloned.1.call-update) | async-done | bytes 262160 | tf_op jit(solution)/shard_map/reduce_scatter | solution.py:211
  226.6 9.7 %all-to-all-start.4 = ((bf16[32,16,256]{2,1,0:T(8,128)(2,1)}), bf16[32,16,256]{2,1,0:T(8,128)(2,1)S(1)}, u32[]{:S(2)}, u32[]{:S(2)}) async-start(bf16[32,16,256]{2,1,0:T(8,128)(2,1)} %bitcast.141), calls=%async_computation.5 | async-start | bytes 524288 | tf_op jit(solution)/shard_map/all_to_all | solution.py:215
  236.3 0.1 copy.112
  236.5 11.0 %all-to-all-done.4 = bf16[32,16,256]{2,1,0:T(8,128)(2,1)S(1)} async-done(((bf16[32,16,256]{2,1,0:T(8,128)(2,1)}), bf16[32,16,256]{2,1,0:T(8,128)(2,1)S(1)}, u32[]{:S(2)}, u32[]{:S(2)}) %all-to-all-start.4) | async-done | bytes 262176 | tf_op jit(solution)/shard_map/all_to_all | solution.py:215
  247.5 1.2 gather_fusion.1
  248.7 0.4 multiply_reduce_fusion
  249.1 0.6 fusion.11
  (49 shorter events, 0.7 us)
Async XLA Ops:
  6.5 150.8 %copy-start = (bf16[1,128,4096]{2,1,0:T(8,128)(2,1)S(1)}, bf16[1,128,4096]{2,1,0:T(8,128)(2,1)}, u32[]{:S(2)}) copy-start(bf16[1,128,4096]{2,1,0:T(8,128)(2,1)} %param.35) | copy-start | bytes 3145732
  13.0 15.5 %copy-start.9 = (f32[64]{0:T(128)S(1)}, f32[64]{0:T(128)}, u32[]{:S(2)}) copy-start(f32[64]{0:T(128)} %param.26) | copy-start | bytes 772
  13.4 26.3 %copy-start.5 = (f32[4,16,64]{2,1,0:T(8,128)S(1)}, f32[4,16,64]{2,1,0:T(8,128)}, u32[]{:S(2)}) copy-start(f32[4,16,64]{2,1,0:T(8,128)} %param.24) | copy-start | bytes 49156
  13.4 26.7 %copy-start.4 = (bf16[64,128]{1,0:T(8,128)(2,1)S(1)}, bf16[64,128]{1,0:T(8,128)(2,1)}, u32[]{:S(2)}) copy-start(bf16[64,128]{1,0:T(8,128)(2,1)} %param.18) | copy-start | bytes 49156
  13.4 26.7 %copy-start.6 = (f32[4,16,64]{2,1,0:T(8,128)S(1)}, f32[4,16,64]{2,1,0:T(8,128)}, u32[]{:S(2)}) copy-start(f32[4,16,64]{2,1,0:T(8,128)} %param.25) | copy-start | bytes 49156
  13.7 26.8 %copy-start.3 = (bf16[64,4096]{1,0:T(8,128)(2,1)S(1)}, bf16[64,4096]{1,0:T(8,128)(2,1)}, u32[]{:S(2)}) copy-start(bf16[64,4096]{1,0:T(8,128)(2,1)} %param.28) | copy-start | bytes 1572868
  15.6 22.2 %all-to-all-start = ((f32[32,1,1024]{2,1,0:T(1,128)}), f32[32,1,1024]{2,1,0:T(1,128)S(1)}, u32[]{:S(2)}, u32[]{:S(2)}) async-start(f32[32,1,1024]{2,1,0:T(1,128)} %reshape.198), calls=%async_computation | async-start | bytes 262144 | tf_op jit(solution)/shard_map/all_to_all | solution.py:12
  39.3 11.8 %copy-start.7 = (s32[128,2]{0,1:T(2,128)S(1)}, s32[128,2]{0,1:T(2,128)}, u32[]{:S(2)}) copy-start(s32[128,2]{0,1:T(2,128)} %param.31) | copy-start | bytes 3076
  42.0 109.2 %copy-start.2 = (bf16[1,4096,128]{2,1,0:T(8,128)(2,1)S(1)}, bf16[1,4096,128]{2,1,0:T(8,128)(2,1)}, u32[]{:S(2)}) copy-start(bf16[1,4096,128]{2,1,0:T(8,128)(2,1)} %param.33) | copy-start | bytes 3145732
  42.0 35.3 %all-to-all-start.1 = ((bf16[16,128,256]{2,1,0:T(8,128)(2,1)}), bf16[16,128,256]{2,1,0:T(8,128)(2,1)S(1)}, u32[]{:S(2)}, u32[]{:S(2)}) async-start(bf16[16,128,256]{2,1,0:T(8,128)(2,1)} %bitcast.68), calls=%async_computation.1 | async-start | bytes 2097152 | tf_op jit(solution)/shard_map/all_to_all | solution.py:61
  79.1 9.3 %all-to-all-start.2 = ((f32[16,1,128]{2,1,0:T(1,128)}), f32[16,1,128]{2,1,0:T(1,128)S(1)}, u32[]{:S(2)}, u32[]{:S(2)}) async-start(f32[16,1,128]{2,1,0:T(1,128)} %broadcast_in_dim.86), calls=%async_computation.2 | async-start | bytes 16384 | tf_op jit(solution)/shard_map/all_to_all | solution.py:12
  84.4 66.9 %all-gather.2.cloned.1.call-start = ((), (), s32[]{:S(2)}) async-start(), calls=%async_computation.6 | async-start | bytes 4456448 | tf_op jit(solution)/shard_map/all_gather | solution.py:205
  105.9 120.7 %reduce-scatter.2.cloned.1.call-start = ((), (), s32[]{:S(2)}) async-start(), calls=%async_computation.7 | async-start | bytes 4456448 | tf_op jit(solution)/shard_map/reduce_scatter | solution.py:211
  151.2 3.6 %copy-start.1 = (bf16[32,16,4096]{2,1,0:T(8,128)(2,1)S(1)}, bf16[32,16,4096]{2,1,0:T(8,128)(2,1)}, u32[]{:S(2)}) copy-start(bf16[32,16,4096]{2,1,0:T(8,128)(2,1)} %all-gather.2.cloned.1.call-done) | copy-start | bytes 12582916
  157.3 3.5 %copy-start.8 = (f32[128,2]{0,1:T(2,128)S(1)}, f32[128,2]{0,1:T(2,128)}, u32[]{:S(2)}) copy-start(f32[128,2]{0,1:T(2,128)} %param.32) | copy-start | bytes 3076
  226.6 20.9 %all-to-all-start.4 = ((bf16[32,16,256]{2,1,0:T(8,128)(2,1)}), bf16[32,16,256]{2,1,0:T(8,128)(2,1)S(1)}, u32[]{:S(2)}, u32[]{:S(2)}) async-start(bf16[32,16,256]{2,1,0:T(8,128)(2,1)} %bitcast.141), calls=%async_computation.5 | async-start | bytes 524288 | tf_op jit(solution)/shard_map/all_to_all | solution.py:215
Sparse Core Ops, SparseCore 0:
  106.1 45.1 all-gather.1
  160.6 65.9 reduce-scatter.1
where the time goes:
time: 257 us
  waiting for transfers between devices  159 us (62%)
  starting transfers between devices  37 us (14%)
  blocking collectives  15.2 us (6%)
  between operations  13.9 us (5%)
  matrix products  12.5 us (5%)
  local copies, waits for them, and re-layouts  9.55 us (4%)
  other arithmetic  9.4 us (4%)
    reduce_scatter x1, waiting for transfers between devices, per_device(): lax.psum_scatter(down_part.astype(f32).astype(jnp.bfloat16), 'tp', scatte...  65.8 us
    all_gather x1, waiting for transfers between devices, per_device(): piece = lax.all_gather(arrived, 'tp', axis=2, tiled=True)  45.2 us
    all_to_all x1, waiting for transfers between devices, sent_and_summed(): lax.all_to_all(in_blocks(array, dim, length), axis, 0, 0, tiled=True)  24.5 us
    all_to_all x2, starting transfers between devices, copy_for_each(): return lax.all_to_all(copies, axis, split_axis=0, concat_axis=0, tiled=True)  18.1 us
    all_to_all x1, blocking collectives, per_device(): lax.all_to_all(dispatch, 'sp', split_axis=0, concat_axis=0, tiled=True)  15.2 us
    all_to_all x2, waiting for transfers between devices, copy_for_each(): return lax.all_to_all(copies, axis, split_axis=0, concat_axis=0, tiled=True)  12.5 us
    all_to_all x1, waiting for transfers between devices, per_device(): lax.all_to_all(expert_out, 'sp', split_axis=0, concat_axis=0, tiled=True)  11 us
    all_to_all x1, starting transfers between devices, per_device(): lax.all_to_all(expert_out, 'sp', split_axis=0, concat_axis=0, tiled=True)  9.71 us
  transfers between devices with their start and end apart: 6, of which 6 were waited for; matrix products, arithmetic and copies ran while one was open for 1% of the time, Pallas kernels for 0%

commit v1 on v0

--- a/solution.py
+++ b/solution.py
@@ -202,7 +202,7 @@
         experts, capacity, d_local
     )
     arrived = lax.all_to_all(dispatch, "sp", split_axis=0, concat_axis=0, tiled=True)
-    piece = lax.all_gather(arrived, "tp", axis=2, tiled=True)
+    piece = jnp.concatenate(lax.all_gather(arrived, "tp"), axis=2)
     gate_part = jnp.einsum("snd,df->snf", piece, gate_w, preferred_element_type=f32)
     up_part = jnp.einsum("snd,df->snf", piece, up_w, preferred_element_type=f32)
     hidden = (jax.nn.silu(gate_part) * up_part).astype(bf16)

time: 257 us -> 249 us (0.969)
  waiting for transfers between devices: 159 us -> 151 us
  matrix products: 12.5 us -> 8.97 us
  local copies, waits for them, and re-layouts: 9.55 us -> 12.4 us
    all_gather x1, waiting for transfers between devices: 45.2 us -> 38.7 us  [per_device(): piece = jnp.concatenate(lax.all_gather(arrived, 'tp'), axis=2)]
    reshape x0 -> x1, local copies, waits for them, and re-layouts: none -> 2.82 us  [per_device(): piece = jnp.concatenate(lax.all_gather(arrived, 'tp'), axis=2)]
where the time goes in v1:
time: 249 us
  waiting for transfers between devices  151 us (61%)
  starting transfers between devices  37.5 us (15%)
  blocking collectives  15.2 us (6%)
  between operations  13.9 us (6%)
  local copies, waits for them, and re-layouts  12.4 us (5%)
  other arithmetic  9.4 us (4%)
  matrix products  8.97 us (4%)
    reduce_scatter x1, waiting for transfers between devices, per_device(): lax.psum_scatter(down_part.astype(f32).astype(jnp.bfloat16), 'tp', scatte...  64.6 us
    all_gather x1, waiting for transfers between devices, per_device(): piece = jnp.concatenate(lax.all_gather(arrived, 'tp'), axis=2)  38.7 us
    all_to_all x1, waiting for transfers between devices, sent_and_summed(): lax.all_to_all(in_blocks(array, dim, length), axis, 0, 0, tiled=True)  24.5 us
    all_to_all x2, starting transfers between devices, copy_for_each(): return lax.all_to_all(copies, axis, split_axis=0, concat_axis=0, tiled=True)  18.1 us
    all_to_all x1, blocking collectives, per_device(): lax.all_to_all(dispatch, 'sp', split_axis=0, concat_axis=0, tiled=True)  15.2 us
    all_to_all x2, waiting for transfers between devices, copy_for_each(): return lax.all_to_all(copies, axis, split_axis=0, concat_axis=0, tiled=True)  12.5 us
    all_to_all x1, waiting for transfers between devices, per_device(): lax.all_to_all(expert_out, 'sp', split_axis=0, concat_axis=0, tiled=True)  11 us
    all_to_all x1, starting transfers between devices, per_device(): lax.all_to_all(expert_out, 'sp', split_axis=0, concat_axis=0, tiled=True)  10.1 us
  transfers between devices with their start and end apart: 6, of which 6 were waited for; matrix products, arithmetic and copies ran while one was open for 1% of the time, Pallas kernels for 0%

profile of v1, /device:TPU:25, one launch (start us, length us, event | category | flops | bytes accessed | tf_op | source)
XLA Modules:
  0.0 248.6 jit_solution(3410195243867221849)
XLA Ops:
  6.5 0.7 exp.13
  7.3 0.8 fusion.57
  8.1 1.1 fusion.42
  9.2 1.1 fusion.46
  10.3 0.9 subtract_add_fusion.6
  11.2 1.0 add_add_fusion.5
  12.2 0.1 subtract_add_fusion.5
  12.3 0.2 add_add_fusion.4
  12.5 0.1 subtract_add_fusion.4
  12.7 0.2 add_add_fusion.3
  12.9 0.1 subtract_add_fusion.3
  13.1 0.2 add_add_fusion.2
  13.3 0.1 subtract_add_fusion.2
  13.4 0.2 add_add_fusion.1
  13.7 0.1 subtract_add_fusion.1
  13.8 0.2 add_add_fusion
  14.0 0.2 multiply_subtract_fusion
  14.2 0.3 slice_reduce_fusion.1
  14.5 0.3 slice_reduce_fusion
  14.8 0.8 reshape.207
  15.6 12.9 %all-to-all-start = ((f32[32,1,1024]{2,1,0:T(1,128)}), f32[32,1,1024]{2,1,0:T(1,128)S(1)}, u32[]{:S(2)}, u32[]{:S(2)}) async-start(f32[32,1,1024]{2,1,0:T(1,128)} %reshape.207), calls=%async_computation | async-start | bytes 262144 | tf_op jit(solution)/shard_map/all_to_all | solution.py:12
  28.6 9.2 %all-to-all-done = f32[32,1,1024]{2,1,0:T(1,128)S(1)} async-done(((f32[32,1,1024]{2,1,0:T(1,128)}), f32[32,1,1024]{2,1,0:T(1,128)S(1)}, u32[]{:S(2)}, u32[]{:S(2)}) %all-to-all-start) | async-done | bytes 131104 | tf_op jit(solution)/shard_map/all_to_all | solution.py:12
  37.9 0.5 broadcast.191
  38.4 1.0 reduce.12
  39.4 0.1 reshape.208
  39.5 0.1 slice_select_fusion.3
  39.8 0.3 fusion.16
  40.1 0.4 fusion.36
  40.5 0.5 convolution_convert_fusion.1
  41.0 1.1 copy.125
  42.1 9.0 %all-to-all-start.1 = ((bf16[16,128,256]{2,1,0:T(8,128)(2,1)}), bf16[16,128,256]{2,1,0:T(8,128)(2,1)S(1)}, u32[]{:S(2)}, u32[]{:S(2)}) async-start(bf16[16,128,256]{2,1,0:T(8,128)(2,1)} %bitcast.73), calls=%async_computation.1 | async-start | bytes 2097152 | tf_op jit(solution)/shard_map/all_to_all | solution.py:61
  51.1 0.1 copy.113
  51.2 0.1 eq.40
  51.3 0.1 reshape.174
  51.5 0.6 reduce-window.6
  52.1 0.2 slice_reduce_fusion.4
  52.4 0.2 fusion.7
  52.6 0.2 select_reduce_fusion
  52.8 24.5 %all-to-all-done.1 = bf16[16,128,256]{2,1,0:T(8,128)(2,1)S(1)} async-done(((bf16[16,128,256]{2,1,0:T(8,128)(2,1)}), bf16[16,128,256]{2,1,0:T(8,128)(2,1)S(1)}, u32[]{:S(2)}, u32[]{:S(2)}) %all-to-all-start.1) | async-done | bytes 1048608 | tf_op jit(solution)/shard_map/all_to_all | solution.py:61
  77.3 0.1 reduce_sum.70
  77.4 0.9 add_convert_fusion
  78.3 0.1 fusion.8
  78.4 0.6 broadcast_in_dim.86
  79.0 5.2 %all-to-all-start.2 = ((f32[16,1,128]{2,1,0:T(1,128)}), f32[16,1,128]{2,1,0:T(1,128)S(1)}, u32[]{:S(2)}, u32[]{:S(2)}) async-start(f32[16,1,128]{2,1,0:T(1,128)} %broadcast_in_dim.86), calls=%async_computation.2 | async-start | bytes 16384 | tf_op jit(solution)/shard_map/all_to_all | solution.py:12
  84.3 0.8 dynamic_slice.7
  85.1 3.2 %all-to-all-done.2 = f32[16,1,128]{2,1,0:T(1,128)S(1)} async-done(((f32[16,1,128]{2,1,0:T(1,128)}), f32[16,1,128]{2,1,0:T(1,128)S(1)}, u32[]{:S(2)}, u32[]{:S(2)}) %all-to-all-start.2) | async-done | bytes 8224 | tf_op jit(solution)/shard_map/all_to_all | solution.py:12
  88.5 2.0 gather_fusion
  90.5 0.1 broadcast_select_fusion
  90.6 15.2 %all_to_all.26 = bf16[32,16,256]{2,1,0:T(8,128)(2,1)} all-to-all(bf16[32,16,256]{2,1,0:T(8,128)(2,1)S(1)} %broadcast_select_fusion), channel_id=1, replica_groups=mesh['sp'=32,'tp'=16] {'sp'}, dimensions={0} | all-to-all | bytes 524288 | tf_op jit(solution)/shard_map/all_to_all | solution.py:204
  105.8 0.2 reduce-scatter.2.cloned.1.call-start
  106.0 38.7 %all-gather.3.cloned.1.call-done = bf16[512,16,256]{2,1,0:T(8,128)(2,1)} async-done(((bf16[32,16,256]{2,1,0:T(8,128)(2,1)}), bf16[512,16,256]{2,1,0:T(8,128)(2,1)}) %all-gather.3.cloned.1.call-update) | async-done | bytes 4194320 | tf_op jit(solution)/shard_map/all_gather | solution.py:205
  144.8 2.8 %copy.122 = bf16[16,32,2,8,256]{4,3,0,2,1:T(8,128)(2,1)S(1)} copy(bf16[16,32,2,8,256]{4,3,2,1,0:T(8,128)(2,1)} %bitcast.105) | data formatting | bytes 8388608 | tf_op jit(solution)/shard_map/reshape | solution.py:205
  147.6 1.2 fusion.5
  148.9 1.3 fusion
  150.2 3.2 %convolution_convert_fusion = bf16[512,4096]{1,0:T(8,128)(2,1)} fusion(bf16[512,128]{1,0:T(8,128)(2,1)S(1)} %bitcast.148, bf16[1,128,4096]{2,1,0:T(8,128)(2,1)S(1)} %copy-done), kind=kOutput, calls=%fused_computation.2 | convolution fusion | flops 538968064 | bytes 5373952 | tf_op jit(solution)/shard_map/dot_general | solution.py:210
  153.4 0.1 copy.118
  153.5 0.1 mul.645
  153.7 64.6 %reduce-scatter.2.cloned.1.call-done = bf16[512,256]{1,0:T(8,128)(2,1)} async-done(((bf16[512,4096]{1,0:T(8,128)(2,1)}), bf16[512,256]{1,0:T(8,128)(2,1)}) %reduce-scatter.2.cloned.1.call-update) | async-done | bytes 262160 | tf_op jit(solution)/shard_map/reduce_scatter | solution.py:211
  218.3 10.1 %all-to-all-start.4 = ((bf16[32,16,256]{2,1,0:T(8,128)(2,1)}), bf16[32,16,256]{2,1,0:T(8,128)(2,1)S(1)}, u32[]{:S(2)}, u32[]{:S(2)}) async-start(bf16[32,16,256]{2,1,0:T(8,128)(2,1)} %bitcast.149), calls=%async_computation.5 | async-start | bytes 524288 | tf_op jit(solution)/shard_map/all_to_all | solution.py:215
  228.4 0.1 copy.119
  228.5 11.0 %all-to-all-done.4 = bf16[32,16,256]{2,1,0:T(8,128)(2,1)S(1)} async-done(((bf16[32,16,256]{2,1,0:T(8,128)(2,1)}), bf16[32,16,256]{2,1,0:T(8,128)(2,1)S(1)}, u32[]{:S(2)}, u32[]{:S(2)}) %all-to-all-start.4) | async-done | bytes 262176 | tf_op jit(solution)/shard_map/all_to_all | solution.py:215
  239.5 1.2 gather_fusion.1
  240.7 0.4 multiply_reduce_fusion
  241.2 0.6 fusion.11
  (50 shorter events, 0.8 us)
Async XLA Ops:
  6.5 143.6 %copy-start = (bf16[1,128,4096]{2,1,0:T(8,128)(2,1)S(1)}, bf16[1,128,4096]{2,1,0:T(8,128)(2,1)}, u32[]{:S(2)}) copy-start(bf16[1,128,4096]{2,1,0:T(8,128)(2,1)} %param.35) | copy-start | bytes 3145732
  13.0 15.5 %copy-start.8 = (f32[64]{0:T(128)S(1)}, f32[64]{0:T(128)}, u32[]{:S(2)}) copy-start(f32[64]{0:T(128)} %param.26) | copy-start | bytes 772
  13.4 26.3 %copy-start.4 = (f32[4,16,64]{2,1,0:T(8,128)S(1)}, f32[4,16,64]{2,1,0:T(8,128)}, u32[]{:S(2)}) copy-start(f32[4,16,64]{2,1,0:T(8,128)} %param.24) | copy-start | bytes 49156
  13.4 26.7 %copy-start.3 = (bf16[64,128]{1,0:T(8,128)(2,1)S(1)}, bf16[64,128]{1,0:T(8,128)(2,1)}, u32[]{:S(2)}) copy-start(bf16[64,128]{1,0:T(8,128)(2,1)} %param.18) | copy-start | bytes 49156
  13.4 26.7 %copy-start.5 = (f32[4,16,64]{2,1,0:T(8,128)S(1)}, f32[4,16,64]{2,1,0:T(8,128)}, u32[]{:S(2)}) copy-start(f32[4,16,64]{2,1,0:T(8,128)} %param.25) | copy-start | bytes 49156
  13.7 26.8 %copy-start.2 = (bf16[64,4096]{1,0:T(8,128)(2,1)S(1)}, bf16[64,4096]{1,0:T(8,128)(2,1)}, u32[]{:S(2)}) copy-start(bf16[64,4096]{1,0:T(8,128)(2,1)} %param.28) | copy-start | bytes 1572868
  15.6 22.2 %all-to-all-start = ((f32[32,1,1024]{2,1,0:T(1,128)}), f32[32,1,1024]{2,1,0:T(1,128)S(1)}, u32[]{:S(2)}, u32[]{:S(2)}) async-start(f32[32,1,1024]{2,1,0:T(1,128)} %reshape.207), calls=%async_computation | async-start | bytes 262144 | tf_op jit(solution)/shard_map/all_to_all | solution.py:12
  39.4 11.7 %copy-start.6 = (s32[128,2]{0,1:T(2,128)S(1)}, s32[128,2]{0,1:T(2,128)}, u32[]{:S(2)}) copy-start(s32[128,2]{0,1:T(2,128)} %param.31) | copy-start | bytes 3076
  42.1 35.2 %all-to-all-start.1 = ((bf16[16,128,256]{2,1,0:T(8,128)(2,1)}), bf16[16,128,256]{2,1,0:T(8,128)(2,1)S(1)}, u32[]{:S(2)}, u32[]{:S(2)}) async-start(bf16[16,128,256]{2,1,0:T(8,128)(2,1)} %bitcast.73), calls=%async_computation.1 | async-start | bytes 2097152 | tf_op jit(solution)/shard_map/all_to_all | solution.py:61
  79.0 9.3 %all-to-all-start.2 = ((f32[16,1,128]{2,1,0:T(1,128)}), f32[16,1,128]{2,1,0:T(1,128)S(1)}, u32[]{:S(2)}, u32[]{:S(2)}) async-start(f32[16,1,128]{2,1,0:T(1,128)} %broadcast_in_dim.86), calls=%async_computation.2 | async-start | bytes 16384 | tf_op jit(solution)/shard_map/all_to_all | solution.py:12
  84.2 60.5 %all-gather.3.cloned.1.call-start = ((), (), s32[]{:S(2)}) async-start(), calls=%async_computation.7 | async-start | bytes 4456448 | tf_op jit(solution)/shard_map/all_gather | solution.py:205
  105.8 112.5 %reduce-scatter.2.cloned.1.call-start = ((), (), s32[]{:S(2)}) async-start(), calls=%async_computation.6 | async-start | bytes 4456448 | tf_op jit(solution)/shard_map/reduce_scatter | solution.py:211
  144.8 2.8 %copy-start.1 = (bf16[1,4096,128]{2,1,0:T(8,128)(2,1)S(1)}, bf16[1,4096,128]{2,1,0:T(8,128)(2,1)}, u32[]{:S(2)}) copy-start(bf16[1,4096,128]{2,1,0:T(8,128)(2,1)} %param.33) | copy-start | bytes 3145732
  147.6 1.3 copy-start.9
  150.2 3.5 %copy-start.7 = (f32[128,2]{0,1:T(2,128)S(1)}, f32[128,2]{0,1:T(2,128)}, u32[]{:S(2)}) copy-start(f32[128,2]{0,1:T(2,128)} %param.32) | copy-start | bytes 3076
  218.3 21.2 %all-to-all-start.4 = ((bf16[32,16,256]{2,1,0:T(8,128)(2,1)}), bf16[32,16,256]{2,1,0:T(8,128)(2,1)S(1)}, u32[]{:S(2)}, u32[]{:S(2)}) async-start(bf16[32,16,256]{2,1,0:T(8,128)(2,1)} %bitcast.149), calls=%async_computation.5 | async-start | bytes 524288 | tf_op jit(solution)/shard_map/all_to_all | solution.py:215
Sparse Core Ops, SparseCore 0:
  105.9 38.7 all-gather.2
  153.5 64.7 reduce-scatter.1
